TPU v7x, 32 devices: a whole 2x2x4 slice. The times are simulated.
32 devices in a mesh: fs: 4 (over y, x), tp: 8 (over z, core).
Axes of the slice: x: 2, y: 2, z: 4, core: 2. Of those that a mesh axis runs over, the one named last changes fastest.
Arguments:
- tokens: bfloat16 [4096, 2048], P(('fs', 'tp')), may hold values from -6 to 6
- gate_weight: bfloat16 [2048, 5632], P('fs', 'tp'), may hold values from -0.125 to 0.125
- up_weight: bfloat16 [2048, 5632], P('fs', 'tp'), may hold values from -0.125 to 0.125
- down_weight: bfloat16 [5632, 2048], P('tp', 'fs'), may hold values from -0.078125 to 0.078125
- grad_out: bfloat16 [4096, 2048], P(('fs', 'tp')), may hold values from -6 to 6
Outputs:
- grad_input: bfloat16 [4096, 2048], P(('fs', 'tp'))
- grad_gate: float32 [2048, 5632], P('fs', 'tp')
- grad_up: float32 [2048, 5632], P('fs', 'tp')
- grad_down: float32 [5632, 2048], P('tp', 'fs')
All inputs are finite; a program needn't handle non-finite values.
Results may differ from a plain program's by a relative error of at most 0.0049.
Values may be sent and summed in bfloat16 or wider, within the bound.
A program may use at most 128 MiB of HBM per device.

v0:
```python
import jax
import jax.numpy as jnp
from jax import lax
from jax.sharding import PartitionSpec as P


def over_rows(left, right):
    return lax.dot_general(
        left, right, (((0,), (0,)), ((), ())), preferred_element_type=jnp.float32
    )


def over_cols(left, right):
    return lax.dot_general(
        left, right, (((1,), (1,)), ((), ())), preferred_element_type=jnp.float32
    )


def body(tokens, gate_weight, up_weight, down_weight, grad_out):
    tok_all, cot_all = (
        lax.all_gather(tokens, "tp", axis=0, tiled=True),
        lax.all_gather(grad_out, "tp", axis=0, tiled=True),
    )
    gate_full, up_full = (
        lax.all_gather(gate_weight, "fs", axis=0, tiled=True),
        lax.all_gather(up_weight, "fs", axis=0, tiled=True),
    )
    down_full = lax.all_gather(down_weight, "fs", axis=1, tiled=True)
    gate_pre = jnp.dot(tok_all, gate_full, preferred_element_type=jnp.float32)
    up_pre = jnp.dot(tok_all, up_full, preferred_element_type=jnp.float32)
    sig_gate = jax.nn.sigmoid(gate_pre)
    active = gate_pre * sig_gate
    hidden = (active * up_pre).astype(jnp.bfloat16)
    d_hidden = over_cols(cot_all, down_full)
    d_gate = (d_hidden * up_pre * sig_gate * (1.0 + gate_pre * (1.0 - sig_gate))).astype(
        jnp.bfloat16
    )
    d_up = (d_hidden * active).astype(jnp.bfloat16)
    grad_input = lax.psum_scatter(
        over_cols(d_gate, gate_full) + over_cols(d_up, up_full),
        "tp",
        scatter_dimension=0,
        tiled=True,
    ).astype(jnp.bfloat16)
    width = gate_full.shape[1]
    summed = lax.psum_scatter(
        jnp.concatenate(
            [over_rows(tok_all, d_gate), over_rows(tok_all, d_up), over_rows(cot_all, hidden)],
            axis=1,
        ),
        "fs",
        scatter_dimension=0,
        tiled=True,
    )
    grad_gate = summed[:, :width]
    grad_up = summed[:, width : 2 * width]
    grad_down = summed[:, 2 * width :].T
    return (grad_input, grad_gate, grad_up, grad_down)


def solution(mesh):
    in_specs = (
        P(("fs", "tp"), None),
        P("fs", "tp"),
        P("fs", "tp"),
        P("tp", "fs"),
        P(("fs", "tp"), None),
    )
    out_specs = (P(("fs", "tp"), None), P("fs", "tp"), P("fs", "tp"), P("tp", "fs"))
    return jax.shard_map(body, mesh=mesh, in_specs=in_specs, out_specs=out_specs, check_vma=False)
```

profile of v0, /device:TPU:8, one launch (start us, length us, event | category | flops | bytes accessed | tf_op | source)
XLA Modules:
  0.0 512.5 jit_solution(16898894607041836768)
XLA Ops:
  7.2 0.7 all-gather.12.cloned.1.call-update
  7.9 0.0 all-gather.10.cloned.1.call-start
  7.9 0.7 all-gather.10.cloned.1.call-update
  8.6 0.0 all-gather.14.cloned.1.call-start
  8.7 0.7 all-gather.14.cloned.1.call-update
  9.4 0.0 all-gather.8.cloned.1.call-start
  9.4 0.5 all-gather.8.cloned.1.call-update
  10.0 0.0 all-gather.6.cloned.1.call-start
  10.0 0.5 all-gather.6.cloned.1.call-update
  10.5 0.0 reduce-scatter.3.cloned.1.call-start
  10.6 41.9 %all-gather.12.cloned.1.call-done = bf16[2048,704]{0,1:T(8,128)(2,1)} async-done(((bf16[512,704]{0,1:T(8,128)(2,1)}), bf16[2048,704]{0,1:T(8,128)(2,1)}) %all-gather.12.cloned.1.call-update) | async-done | bytes 2883600 | tf_op jit(solution)/shard_map/all_gather | solution.py:26
  52.5 47.2 %all-gather.10.cloned.1.call-done = bf16[1024,2048]{1,0:T(8,128)(2,1)} async-done(((bf16[128,2048]{1,0:T(8,128)(2,1)}), bf16[1024,2048]{1,0:T(8,128)(2,1)}) %all-gather.10.cloned.1.call-update) | async-done | bytes 4194320 | tf_op jit(solution)/shard_map/all_gather | solution.py:21
  99.8 7.8 %fusion.3 = f32[1024,704]{0,1:T(8,128)} fusion(bf16[1024,2048]{1,0:T(8,128)(2,1)} %all-gather.10.cloned.1.call-done, bf16[2048,704]{0,1:T(8,128)(2,1)} %all-gather.12.cloned.1.call-done), kind=kOutput, calls=%fused_computation.12 | convolution fusion | flops 2952790016 | bytes 9961472 | tf_op jit(solution)/shard_map/dot_general | solution.py:30
  107.6 35.7 %all-gather.14.cloned.1.call-done = bf16[2048,704]{0,1:T(8,128)(2,1)} async-done(((bf16[512,704]{0,1:T(8,128)(2,1)}), bf16[2048,704]{0,1:T(8,128)(2,1)}) %all-gather.14.cloned.1.call-update) | async-done | bytes 2883600 | tf_op jit(solution)/shard_map/all_gather | solution.py:25
  143.2 7.9 %fusion.4 = f32[1024,704]{0,1:T(8,128)} fusion(bf16[1024,2048]{1,0:T(8,128)(2,1)} %all-gather.10.cloned.1.call-done, bf16[2048,704]{0,1:T(8,128)(2,1)} %all-gather.14.cloned.1.call-done), kind=kOutput, calls=%fused_computation.13 | convolution fusion | flops 2952790016 | bytes 9961472 | tf_op jit(solution)/shard_map/dot_general | solution.py:29
  151.2 35.3 %all-gather.8.cloned.1.call-done = bf16[704,2048]{1,0:T(8,128)(2,1)} async-done(((bf16[704,512]{1,0:T(8,128)(2,1)}), bf16[704,2048]{1,0:T(8,128)(2,1)}) %all-gather.8.cloned.1.call-update) | async-done | bytes 2883600 | tf_op jit(solution)/shard_map/all_gather | solution.py:28
  186.5 47.1 %all-gather.6.cloned.1.call-done = bf16[1024,2048]{1,0:T(8,128)(2,1)} async-done(((bf16[128,2048]{1,0:T(8,128)(2,1)}), bf16[1024,2048]{1,0:T(8,128)(2,1)}) %all-gather.6.cloned.1.call-update) | async-done | bytes 4194320 | tf_op jit(solution)/shard_map/all_gather | solution.py:22
  233.6 8.6 %multiply_convert_fusion.1 = (bf16[1024,704]{0,1:T(8,128)(2,1)S(1)}, bf16[1024,704]{0,1:T(8,128)(2,1)S(1)}) fusion(f32[1024,704]{0,1:T(8,128)} %fusion.4, f32[1024,704]{0,1:T(8,128)} %fusion.3, bf16[1024,2048]{1,0:T(8,128)(2,1)} %all-gather.6.cloned.1.call-done, bf16[704,2048]{1,0:T(8,128)(2,1)} %all-gather.8.cloned.1.call-done), kind=kOutput, calls=%fused_computation.6 | convolution fusion | flops 2962161664 | bytes 15728640 | tf_op jit(solution)/shard_map/dot_general | solution.py:14
  242.3 3.5 fusion.5
  245.8 6.1 %convolution_add_fusion = f32[1024,2048]{1,0:T(8,128)} fusion(f32[1024,2048]{1,0:T(8,128)S(1)} %fusion.5, bf16[1024,704]{0,1:T(8,128)(2,1)S(1)} %get-tuple-element.4, bf16[2048,704]{0,1:T(8,128)(2,1)S(1)} %copy-done.2), kind=kOutput, calls=%fused_computation.1 | convolution fusion | flops 2954887168 | bytes 21102592 | tf_op jit(solution)/shard_map/dot_general | solution.py:14
  251.9 0.0 reduce-scatter.5.cloned.1.call-start
  252.0 1.3 copy-done.5
  253.3 5.1 convolution_bitcast_fusion.1
  258.4 3.2 convolution_bitcast_fusion.2
  261.6 0.1 copy-done.8
  261.7 0.8 copy-done.9
  262.5 3.2 convolution_bitcast_fusion
  265.8 6.5 %pad_maximum_fusion = f32[2048,2112]{0,1:T(8,128)} fusion(f32[2048,704]{0,1:T(8,128)S(1)} %convolution_bitcast_fusion, f32[2048,704]{0,1:T(8,128)S(1)} %convolution_bitcast_fusion.1, f32[2048,704]{0,1:T(8,128)S(1)} %convolution_bitcast_fusion.2), kind=kLoop, calls=%fused_computation | loop fusion | flops 8650752 | bytes 34603008 | tf_op jit(solution)/shard_map/concatenate | solution.py:47
  272.3 66.6 %reduce-scatter.3.cloned.1.call-done = f32[128,2048]{1,0:T(8,128)} async-done(((f32[1024,2048]{1,0:T(8,128)}), f32[128,2048]{1,0:T(8,128)}) %reduce-scatter.3.cloned.1.call-update) | async-done | bytes 1048592 | tf_op jit(solution)/shard_map/reduce_scatter | solution.py:39
  338.9 2.1 convert_element_type.14
  341.0 160.3 %reduce-scatter.5.cloned.1.call-done = f32[512,2112]{0,1:T(8,128)} async-done(((f32[2048,2112]{0,1:T(8,128)}), f32[512,2112]{0,1:T(8,128)}) %reduce-scatter.5.cloned.1.call-update) | async-done | bytes 4325392 | tf_op jit(solution)/shard_map/reduce_scatter | solution.py:46
  501.3 4.4 slice_bitcast_fusion
  (20 shorter events, 0.1 us)
Async XLA Ops:
  7.2 45.4 %all-gather.12.cloned.1.call-start = ((), (), s32[]{:S(2)}) async-start(), calls=%async_computation.5 | async-start | bytes 3604480 | tf_op jit(solution)/shard_map/all_gather | solution.py:26
  7.9 91.9 %all-gather.10.cloned.1.call-start = ((), (), s32[]{:S(2)}) async-start(), calls=%async_computation.4 | async-start | bytes 4718592 | tf_op jit(solution)/shard_map/all_gather | solution.py:21
  8.6 134.6 %all-gather.14.cloned.1.call-start = ((), (), s32[]{:S(2)}) async-start(), calls=%async_computation.6 | async-start | bytes 3604480 | tf_op jit(solution)/shard_map/all_gather | solution.py:25
  9.4 177.1 %all-gather.8.cloned.1.call-start = ((), (), s32[]{:S(2)}) async-start(), calls=%async_computation.3 | async-start | bytes 3604480 | tf_op jit(solution)/shard_map/all_gather | solution.py:28
  10.0 223.6 %all-gather.6.cloned.1.call-start = ((), (), s32[]{:S(2)}) async-start(), calls=%async_computation.2 | async-start | bytes 4718592 | tf_op jit(solution)/shard_map/all_gather | solution.py:22
  10.5 328.3 %reduce-scatter.3.cloned.1.call-start = ((), (), s32[]{:S(2)}) async-start(), calls=%async_computation.7 | async-start | bytes 9437184 | tf_op jit(solution)/shard_map/reduce_scatter | solution.py:39
  151.2 91.1 %copy-start.3 = (bf16[2048,704]{0,1:T(8,128)(2,1)S(1)}, bf16[2048,704]{0,1:T(8,128)(2,1)}, u32[]{:S(2)}) copy-start(bf16[2048,704]{0,1:T(8,128)(2,1)} %all-gather.14.cloned.1.call-done) | copy-start | bytes 8650756
  242.2 3.6 copy-start.6
  242.2 3.6 copy-start.4
  242.3 3.6 copy-start.2
  251.9 1.4 copy-start.5
  251.9 6.4 %copy-start.7 = (bf16[1024,704]{0,1:T(8,128)(2,1)S(1)}, bf16[1024,704]{0,1:T(8,128)(2,1)}, u32[]{:S(2)}) copy-start(bf16[1024,704]{0,1:T(8,128)(2,1)} %copy-done.6) | copy-start | bytes 4325380
  251.9 249.3 %reduce-scatter.5.cloned.1.call-start = ((), (), s32[]{:S(2)}) async-start(), calls=%async_computation.8 | async-start | bytes 21626880 | tf_op jit(solution)/shard_map/reduce_scatter | solution.py:46
  253.3 5.1 copy-start
  258.4 3.2 copy-start.1
  258.4 3.3 copy-start.8
  258.4 4.1 copy-start.9
Sparse Core Ops, SparseCore 0:
  9.8 42.6 all-gather.11
  54.1 45.6 all-gather.9
  101.6 41.5 all-gather.13
  144.9 41.5 all-gather.7
  187.9 45.6 all-gather.5
  252.1 86.7 reduce-scatter.2
  342.0 159.2 reduce-scatter.4
where the time goes:
time: 514 us; the launch traced here: 513 us
  waiting for transfers between devices  437 us (85%)
  matrix products  45.4 us (9%)
  between operations  14.3 us (3%)
  other arithmetic  8.6 us (2%)
  local copies, waits for them, and re-layouts  6.61 us (1%)
    reduce_scatter x1, waiting for transfers between devices, body(): lax.psum_scatter(jnp.concatenate([over_rows(tok_all, d_gate), over_rows(t...  160 us
    reduce_scatter x1, waiting for transfers between devices, body(): lax.psum_scatter(over_cols(d_gate, gate_full) + over_cols(d_up, up_full),...  66.6 us
    all_gather x1, waiting for transfers between devices, body(): lax.all_gather(tokens, 'tp', axis=0, tiled=True)  47.2 us
    all_gather x1, waiting for transfers between devices, body(): lax.all_gather(grad_out, 'tp', axis=0, tiled=True)  47.1 us
    all_gather x1, waiting for transfers between devices, body(): lax.all_gather(up_weight, 'fs', axis=0, tiled=True)  41.9 us
    all_gather x1, waiting for transfers between devices, body(): lax.all_gather(gate_weight, 'fs', axis=0, tiled=True)  35.7 us
    all_gather x1, waiting for transfers between devices, body(): down_full = lax.all_gather(down_weight, 'fs', axis=1, tiled=True)  35.3 us
    dot_general x3, matrix products, over_cols(): lax.dot_general(left, right, (((1,), (1,)), ((), ())), preferred_element_...  18.2 us
  transfers between devices with their start and end apart: 7, of which 7 were waited for; matrix products, arithmetic and copies ran while one was open for 7% of the time, Pallas kernels for 0%

commit v1 on v0

v1 whole, which is shorter than its diff:
```python
import functools

import jax
import jax.numpy as jnp
from jax import lax
from jax.experimental import pallas as pl
from jax.experimental.pallas import tpu as pltpu
from jax.sharding import PartitionSpec as P

MESH = pl.DeviceIdType.MESH
CORES = 2


def over_rows(left, right, out=jnp.float32):
    return lax.dot_general(
        left, right, (((0,), (0,)), ((), ())), preferred_element_type=jnp.float32
    ).astype(out)


def over_cols(left, right):
    return lax.dot_general(
        left, right, (((1,), (1,)), ((), ())), preferred_element_type=jnp.float32
    )


def orders_of(n_fs):
    bits = [1 << i for i in range(n_fs.bit_length() - 1)]
    return (bits, bits[::-1])


def first_bit(order, mask):
    return next(i for i, bit in enumerate(order) if mask & bit)


def greet(n_fs, depth, fs, tp, z):
    barrier = pltpu.get_barrier_semaphore()
    bits = orders_of(n_fs)[0]

    def hello(fs_id, tp_id):
        pl.semaphore_signal(barrier, inc=1, device_id=(fs_id, tp_id), device_id_type=MESH)

    for bit in bits:
        hello(fs ^ bit, tp)
    hello(fs, tp ^ 1)

    @pl.when(z > 0)
    def _():
        hello(fs, tp - CORES)

    @pl.when(z < depth - 1)
    def _():
        hello(fs, tp + CORES)

    ends = (z > 0).astype(jnp.int32) + (z < depth - 1).astype(jnp.int32)
    pl.semaphore_wait(barrier, len(bits) + 1 + ends)


def gather_kernel(n_fs, n_tp, *refs):
    ins, outs = refs[:5], refs[5:10]
    w_send, w_recv, z_send, z_recv, c_send, c_recv, l_sem = refs[10:]
    fs, tp = lax.axis_index("fs"), lax.axis_index("tp")
    depth = n_tp // CORES
    z = tp // CORES
    orders = orders_of(n_fs)
    phases = len(orders[0])
    weights = ((ins[1], outs[1], 0), (ins[2], outs[2], 0), (ins[3], outs[3], 1))
    rows = ((ins[0], outs[0]), (ins[4], outs[4]))
    greet(n_fs, depth, fs, tp, z)

    def w_block(array, split, owner):
        ref, out, axis = weights[array]
        half = ref.shape[0] // 2
        if axis == 0:
            own = ref.at[pl.ds(split * half, half), :]
            there = out.at[pl.ds(pl.multiple_of(owner * ref.shape[0] + split * half, half), half), :]
        else:
            own = ref.at[pl.ds(split * half, half), :]
            cols = ref.shape[1]
            there = out.at[pl.ds(split * half, half), pl.ds(pl.multiple_of(owner * cols, cols), cols)]
        return own, there

    def w_copy(array, split, phase, mask):
        own, there = w_block(array, split, fs ^ mask)
        order = orders[split]
        slot = (array, split, (1 << phase) - 1 + sum(1 << i for i in range(phase) if mask & order[i]))
        return pltpu.make_async_remote_copy(
            src_ref=own if mask == 0 else there,
            dst_ref=there,
            send_sem=w_send.at[slot],
            recv_sem=w_recv.at[slot],
            device_id=(fs ^ order[phase], tp),
            device_id_type=MESH,
        )

    def r_block(array, owner):
        ref, out = rows[array]
        n = ref.shape[0]
        return out.at[pl.ds(pl.multiple_of(owner * n, n), n), :]

    def z_copy(array, way, step):
        sign = 1 if way == 0 else -1
        there = r_block(array, tp - sign * step * CORES)
        return pltpu.make_async_remote_copy(
            src_ref=rows[array][0] if step == 0 else there,
            dst_ref=there,
            send_sem=z_send.at[array, way, step],
            recv_sem=z_recv.at[array, way, step],
            device_id=(fs, tp + sign * CORES),
            device_id_type=MESH,
        )

    def sends(way, step):
        if way == 0:
            return jnp.logical_and(z - step >= 0, z < depth - 1)
        return jnp.logical_and(z + step <= depth - 1, z > 0)

    def arrives(way, step):
        return z - 1 - step >= 0 if way == 0 else z + 1 + step <= depth - 1

    def c_copy(array, way, step):
        sign = 1 if way == 0 else -1
        there = r_block(array, tp - sign * (step + 1) * CORES)
        slot = (array, way, step + 1)
        return pltpu.make_async_remote_copy(
            src_ref=rows[array][0] if step == -1 else there,
            dst_ref=there,
            send_sem=c_send.at[slot],
            recv_sem=c_recv.at[slot],
            device_id=(fs, tp ^ 1),
            device_id_type=MESH,
        )

    for array in range(2):
        for way in range(2):

            @pl.when(sends(way, 0))
            def _():
                z_copy(array, way, 0).start()

    for phase in range(phases):
        for array in range(3):
            for split in range(2):
                w_copy(array, split, phase, 0).start()
    for array in range(2):
        c_copy(array, 0, -1).start()
    local = []
    for array in range(3):
        for split in range(2):
            own, there = w_block(array, split, fs)
            local.append((own, there))
    for array in range(2):
        local.append((rows[array][0], r_block(array, tp)))
    local = [pltpu.make_async_copy(a, b, l_sem.at[i]) for i, (a, b) in enumerate(local)]
    for copy in local:
        copy.start()

    def w_event(array, phase, index):
        for split in range(2):
            order = orders[split]
            mask = sum(order[i] for i in range(phase) if index & (1 << i))
            w_copy(array, split, phase, mask).wait_recv()
            got = mask | order[phase]
            for later in range(phase + 1, phases):
                w_copy(array, split, later, got).start()

    def z_event(array, way, step):
        @pl.when(arrives(way, step))
        def _():
            z_copy(array, way, step).wait_recv()
            c_copy(array, way, step).start()

        if step + 1 < depth - 1:

            @pl.when(sends(way, step + 1))
            def _():
                z_copy(array, way, step + 1).start()

    w_events = [
        functools.partial(w_event, array, phase, index)
        for phase in range(phases)
        for index in range(1 << phase)
        for array in range(3)
    ]
    z_events = [
        [functools.partial(z_event, array, way, step) for way in range(2)]
        for step in range(depth - 1)
        for array in range(2)
    ]
    for i in range(max(len(w_events), len(z_events))):
        if i < len(w_events):
            w_events[i]()
        if i < len(z_events):
            for event in z_events[i]:
                event()

    for copy in local:
        copy.wait()
    for array in range(2):
        c_copy(array, 0, -1).wait_send()
        c_copy(array, 0, -1).wait_recv()
        for way in range(2):
            for step in range(depth - 1):

                @pl.when(sends(way, step))
                def _():
                    z_copy(array, way, step).wait_send()

                @pl.when(arrives(way, step))
                def _():
                    c_copy(array, way, step).wait_send()
                    c_copy(array, way, step).wait_recv()

    for array in range(3):
        for split in range(2):
            order = orders[split]
            for phase in range(phases):
                for index in range(1 << phase):
                    mask = sum(order[i] for i in range(phase) if index & (1 << i))
                    w_copy(array, split, phase, mask).wait_send()


def gather_all(n_fs, n_tp, *ins):
    tokens, gate, up, down, cot = ins
    depth = n_tp // CORES
    any_spec = pl.BlockSpec(memory_space=pl.ANY)
    vmem = pl.BlockSpec(memory_space=pltpu.VMEM)
    full = lambda a, axis, n: jax.ShapeDtypeStruct(
        tuple(s * n if i == axis else s for i, s in enumerate(a.shape)), a.dtype
    )
    dma = pltpu.SemaphoreType.DMA
    return pl.pallas_call(
        functools.partial(gather_kernel, n_fs, n_tp),
        out_shape=(
            full(tokens, 0, n_tp),
            full(gate, 0, n_fs),
            full(up, 0, n_fs),
            full(down, 1, n_fs),
            full(cot, 0, n_tp),
        ),
        in_specs=[vmem] * 5,
        out_specs=[any_spec] * 5,
        scratch_shapes=[
            dma((3, 2, n_fs - 1)),
            dma((3, 2, n_fs - 1)),
            dma((2, 2, max(depth - 1, 1))),
            dma((2, 2, max(depth - 1, 1))),
            dma((2, 2, depth)),
            dma((2, 2, depth)),
            dma((8,)),
        ],
        compiler_params=pltpu.CompilerParams(collective_id=0, has_side_effects=True),
        name="gather",
    )(*ins)


def scatter_kernel(n_fs, n_tp, *refs):
    gi_ref, *w_refs = refs[:4]
    gi_out, *w_outs = refs[4:8]
    stages, recvs = refs[8:11], refs[11:14]
    c_buf, z_stage, z_buf = refs[14:17]
    w_send, w_recv, z_send, z_recv, c_send, c_recv = refs[17:]
    fs, tp = lax.axis_index("fs"), lax.axis_index("tp")
    depth = n_tp // CORES
    z, core = tp // CORES, tp % CORES
    orders = orders_of(n_fs)
    phases = len(orders[0])
    axes = (0, 0, 1)
    f32 = jnp.float32
    greet(n_fs, depth, fs, tp, z)

    def w_own(array, split, mask):
        out, axis = w_outs[array], axes[array]
        half = out.shape[0] // 2
        owner = fs ^ mask
        if axis == 0:
            start = pl.multiple_of(owner * out.shape[0] + split * half, half)
            return w_refs[array].at[pl.ds(start, half), :]
        cols = out.shape[1]
        return w_refs[array].at[
            pl.ds(split * half, half), pl.ds(pl.multiple_of(owner * cols, cols), cols)
        ]

    def compact(order, mask):
        return sum(1 << i for i, bit in enumerate(order) if mask & bit)

    def w_copy(array, split, mask):
        order = orders[split]
        phase = first_bit(order, mask)
        slot = compact(order, mask) - 1
        src = w_own(array, split, mask) if phase == 0 else stages[array].at[split, slot]
        return pltpu.make_async_remote_copy(
            src_ref=src,
            dst_ref=recvs[array].at[split, slot],
            send_sem=w_send.at[array, split, slot],
            recv_sem=w_recv.at[array, split, slot],
            device_id=(fs ^ order[phase], tp),
            device_id_type=MESH,
        )

    def w_sum(array, split, mask):
        order = orders[split]
        total = w_own(array, split, mask)[...].astype(f32)
        limit = phases if mask == 0 else first_bit(order, mask)
        for phase in range(limit):
            sent = mask | order[phase]
            w_copy(array, split, sent).wait_recv()
            total += recvs[array][split, compact(order, sent) - 1].astype(f32)
        return total

    n = gi_out.shape[0]

    def g_rows(target, which):
        return pl.ds(pl.multiple_of((target * CORES + which) * n, n), n)

    def c_copy(target):
        return pltpu.make_async_remote_copy(
            src_ref=gi_ref.at[g_rows(target, 1 - core), :],
            dst_ref=c_buf.at[target],
            send_sem=c_send.at[target],
            recv_sem=c_recv.at[target],
            device_id=(fs, tp ^ 1),
            device_id_type=MESH,
        )

    def z_target(way, step):
        return depth - 1 - step if way == 0 else step

    def z_copy(way, step):
        return pltpu.make_async_remote_copy(
            src_ref=z_stage.at[way, step],
            dst_ref=z_buf.at[way, step],
            send_sem=z_send.at[way, step],
            recv_sem=z_recv.at[way, step],
            device_id=(fs, tp + CORES if way == 0 else tp - CORES),
            device_id_type=MESH,
        )

    def sends(way, step):
        t = z_target(way, step)
        return t > z if way == 0 else t < z

    def arrives(way, step):
        t = z_target(way, step)
        return jnp.logical_and(z > 0, t >= z) if way == 0 else jnp.logical_and(z < depth - 1, t <= z)

    targets = []
    for i in range(depth):
        t = depth - 1 - i // 2 if i % 2 == 0 else i // 2
        targets.append(t)
    for t in targets:
        c_copy(t).start()

    for array in range(3):
        for split in range(2):
            order = orders[split]
            masks = [m for m in range(1, n_fs) if m & order[0]]
            for mask in sorted(masks, key=lambda m: -compact(order, m)):
                w_copy(array, split, mask).start()

    both = c_buf
    for t in targets:
        c_copy(t).wait_recv()
        both[t] = (
            both[t].astype(f32) + gi_ref[g_rows(t, core), :].astype(f32)
        ).astype(both.dtype)

    def z_event(way, step):
        t = z_target(way, step)

        @pl.when(arrives(way, step))
        def _():
            z_copy(way, step).wait_recv()

        @pl.when(sends(way, step))
        def _():
            @pl.when(arrives(way, step))
            def _():
                z_stage[way, step] = (
                    both[t].astype(f32) + z_buf[way, step].astype(f32)
                ).astype(z_stage.dtype)

            @pl.when(jnp.logical_not(arrives(way, step)))
            def _():
                z_stage[way, step] = both[t]

            z_copy(way, step).start()

    def w_event(array, mask):
        for split in range(2):
            order = orders[split]
            real = sum(bit for i, bit in enumerate(order) if mask & (1 << i))
            slot = mask - 1
            stages[array][split, slot] = w_sum(array, split, real).astype(stages[array].dtype)
            w_copy(array, split, real).start()

    def w_finish(array):
        half = w_outs[array].shape[0] // 2
        for split in range(2):
            w_outs[array][pl.ds(split * half, half), :] = w_sum(array, split, 0)

    later = [m for m in range(1, n_fs) if not m & 1]
    later = sorted(later, key=lambda m: ((m & -m), -m))
    w_events = [functools.partial(w_event, array, mask) for array in range(3) for mask in later]
    z_events = [
        functools.partial(z_event, way, step) for step in range(depth - 1) for way in range(2)
    ]
    per = -(-len(z_events) // max(len(w_events), 1))
    for i in range(max(len(w_events), -(-len(z_events) // per))):
        for event in z_events[i * per : (i + 1) * per]:
            event()
        if i < len(w_events):
            w_events[i]()

    total = both[z].astype(f32)
    zero = jnp.zeros_like(total)
    from_left = z_buf[0, jnp.clip(depth - 1 - z, 0, depth - 2)].astype(f32)
    from_right = z_buf[1, jnp.clip(z, 0, depth - 2)].astype(f32)
    total += jnp.where(z > 0, from_left, zero)
    total += jnp.where(z < depth - 1, from_right, zero)
    gi_out[...] = total.astype(gi_out.dtype)

    for array in range(3):
        w_finish(array)

    for t in targets:
        c_copy(t).wait_send()
    for way in range(2):
        for step in range(depth - 1):

            @pl.when(sends(way, step))
            def _():
                z_copy(way, step).wait_send()

    for array in range(3):
        for split in range(2):
            for mask in range(1, n_fs):
                w_copy(array, split, mask).wait_send()


def scatter_all(n_fs, n_tp, gi, gg, gu, gd):
    depth = n_tp // CORES
    f32 = jnp.float32
    vmem = pl.BlockSpec(memory_space=pltpu.VMEM)
    dma = pltpu.SemaphoreType.DMA
    shapes = (
        (gg.shape[0] // n_fs, gg.shape[1]),
        (gu.shape[0] // n_fs, gu.shape[1]),
        (gd.shape[0], gd.shape[1] // n_fs),
    )
    n, width = gi.shape[0] // n_tp, gi.shape[1]
    slots = [pltpu.VMEM((2, n_fs - 1, s[0] // 2, s[1]), gi.dtype) for s in shapes]
    return pl.pallas_call(
        functools.partial(scatter_kernel, n_fs, n_tp),
        out_shape=(jax.ShapeDtypeStruct((n, width), gi.dtype),)
        + tuple(jax.ShapeDtypeStruct(s, f32) for s in shapes),
        in_specs=[vmem] * 4,
        out_specs=[vmem] * 4,
        scratch_shapes=slots
        + slots
        + [
            pltpu.VMEM((depth, n, width), gi.dtype),
            pltpu.VMEM((2, depth - 1, n, width), gi.dtype),
            pltpu.VMEM((2, depth - 1, n, width), gi.dtype),
            dma((3, 2, n_fs - 1)),
            dma((3, 2, n_fs - 1)),
            dma((2, depth - 1)),
            dma((2, depth - 1)),
            dma((depth,)),
            dma((depth,)),
        ],
        compiler_params=pltpu.CompilerParams(
            collective_id=1, has_side_effects=True, vmem_limit_bytes=60 * 1024 * 1024
        ),
        name="scatter",
    )(gi, gg, gu, gd)


def body(n_fs, n_tp, tokens, gate_weight, up_weight, down_weight, grad_out):
    bf16 = tokens.dtype
    tok_all, gate_full, up_full, down_full, cot_all = gather_all(
        n_fs, n_tp, tokens, gate_weight, up_weight, down_weight, grad_out
    )
    gate_pre = jnp.dot(tok_all, gate_full, preferred_element_type=jnp.float32)
    up_pre = jnp.dot(tok_all, up_full, preferred_element_type=jnp.float32)
    sig_gate = jax.nn.sigmoid(gate_pre)
    active = gate_pre * sig_gate
    hidden = (active * up_pre).astype(bf16)
    d_hidden = over_cols(cot_all, down_full)
    d_gate = (d_hidden * up_pre * sig_gate * (1.0 + gate_pre * (1.0 - sig_gate))).astype(bf16)
    d_up = (d_hidden * active).astype(bf16)
    grad_input = (over_cols(d_gate, gate_full) + over_cols(d_up, up_full)).astype(bf16)
    return scatter_all(
        n_fs,
        n_tp,
        grad_input,
        over_rows(tok_all, d_gate, bf16),
        over_rows(tok_all, d_up, bf16),
        over_rows(hidden, cot_all, bf16),
    )


def solution(mesh):
    in_specs = (
        P(("fs", "tp"), None),
        P("fs", "tp"),
        P("fs", "tp"),
        P("tp", "fs"),
        P(("fs", "tp"), None),
    )
    out_specs = (P(("fs", "tp"), None), P("fs", "tp"), P("fs", "tp"), P("tp", "fs"))
    return jax.shard_map(
        functools.partial(body, mesh.shape["fs"], mesh.shape["tp"]),
        mesh=mesh,
        in_specs=in_specs,
        out_specs=out_specs,
        check_vma=False,
    )
```

time: 514 us -> 267 us (0.52)
  waiting for transfers between devices: 437 us -> 0 us
  Pallas kernels: 0 us -> 210 us
  between operations: 14.3 us -> 0.82 us
  local copies, waits for them, and re-layouts: 6.61 us -> 18.6 us
  other arithmetic: 8.6 us -> 0 us
  matrix products: 45.4 us -> 37.3 us
    reduce_scatter x2 -> x0, waiting for transfers between devices: 227 us -> none  [the longest x1 160 us: body(): lax.psum_scatter(jnp.concatenate([over_rows(tok_all, d_gate), over_rows(t...]
    pallas_call x0 -> x2, Pallas kernels: none -> 210 us  [the longest x1 130 us: scatter_all(): pl.pallas_call(functools.partial(scatter_kernel, n_fs, n_tp), out_shape=(...]
    all_gather x5 -> x0, waiting for transfers between devices: 207 us -> none  [the longest x1 47.2 us: body(): lax.all_gather(tokens, 'tp', axis=0, tiled=True)]
    convert_element_type x0 -> x2, local copies, waits for them, and re-layouts: none -> 7.46 us  [over_rows(): return lax.dot_general(left, right, (((0,), (0,)), ((), ())), preferred_e...]
    concatenate x1 -> x0, other arithmetic: 6.52 us -> none  [body(): jnp.concatenate([over_rows(tok_all, d_gate), over_rows(tok_all, d_up), ov...]
  transfers between devices with their start and end apart: 7 -> 0, of which waited for: 7 -> 0; matrix products, arithmetic and copies ran while one was open for 7% -> 0% of each run, Pallas kernels for 0% -> 0%
where the time goes in v1:
time: 267 us
  Pallas kernels  210 us (79%)
  matrix products  37.3 us (14%)
  local copies, waits for them, and re-layouts  18.6 us (7%)
    pallas_call x1, Pallas kernels, scatter_all(): pl.pallas_call(functools.partial(scatter_kernel, n_fs, n_tp), out_shape=(...  130 us
    pallas_call x1, Pallas kernels, gather_all(): pl.pallas_call(functools.partial(gather_kernel, n_fs, n_tp), out_shape=(f...  80.2 us
    dot_general x3, matrix products, over_cols(): lax.dot_general(left, right, (((1,), (1,)), ((), ())), preferred_element_...  15.2 us
    dot_general x3, matrix products, over_rows(): lax.dot_general(left, right, (((0,), (0,)), ((), ())), preferred_element_...  12.7 us
    convert_element_type x2, local copies, waits for them, and re-layouts, over_rows(): return lax.dot_general(left, right, (((0,), (0,)), ((), ())), preferred_e...  7.46 us
    unnamed x26, local copies, waits for them, and re-layouts  6.47 us
    dot_general x1, matrix products, body(): up_pre = jnp.dot(tok_all, up_full, preferred_element_type=jnp.float32)  6.11 us

profile of v1, /device:TPU:8, one launch (start us, length us, event | category | flops | bytes accessed | tf_op | source)
XLA Modules:
  0.0 267.2 jit_solution(17983723745009055509)
XLA Ops:
  0.6 2.3 copy.15.refs_1_
  2.9 2.3 copy.16.refs_2_
  5.2 80.2 %gather.1 = (bf16[1024,2048]{1,0:T(8,128)(2,1)}, bf16[2048,704]{1,0:T(8,128)(2,1)}, bf16[2048,704]{1,0:T(8,128)(2,1)}, bf16[704,2048]{1,0:T(8,128)(2,1)}, bf16[1024,2048]{1,0:T(8,128)(2,1)}) custom-call(bf16[128,2048]{1,0:T(8,128)(2,1)} %refs_0_.1, bf16[512,704]{1,0:T(8,128)(2,1)} %copy.15.refs_1_, bf16[512,704]{1,0:T(8,128)(2,1)} %copy.16.refs_2_, ...), custom_call_target="tpu_custom_call" | custom-call | tf_op jit(solution)/shard_map/gather/pallas_call | solution.py:231
  85.4 0.0 copy-start.3
  85.4 0.0 copy-start.6
  85.4 6.1 %fusion.3 = f32[1024,704]{0,1:T(8,128)S(1)} fusion(bf16[1024,2048]{1,0:T(8,128)(2,1)} %get-tuple-element.11, bf16[2048,704]{1,0:T(8,128)(2,1)} %get-tuple-element.12), kind=kOutput, calls=%fused_computation.10 | convolution fusion | flops 2952790016 | bytes 9961472 | tf_op jit(solution)/shard_map/dot_general | solution.py:484
  91.5 0.0 copy-done.3
  91.5 0.0 copy-done.6
  91.5 0.0 copy-start.4
  91.5 0.0 copy-start.7
  91.5 3.3 %fusion.4 = f32[1024,704]{0,1:T(8,128)S(1)} fusion(bf16[1024,2048]{1,0:T(8,128)(2,1)S(1)} %copy-done.3, bf16[2048,704]{1,0:T(8,128)(2,1)S(1)} %copy-done.6), kind=kOutput, calls=%fused_computation.11 | convolution fusion | flops 2952790016 | bytes 9961472 | tf_op jit(solution)/shard_map/dot_general | solution.py:483
  94.9 0.0 copy-done.4
  94.9 0.0 copy-done.7
  94.9 4.0 %multiply_convert_fusion.1 = (bf16[1024,704]{0,1:T(8,128)(2,1)S(1)}, bf16[1024,704]{0,1:T(8,128)(2,1)S(1)}) fusion(f32[1024,704]{0,1:T(8,128)S(1)} %fusion.4, f32[1024,704]{0,1:T(8,128)S(1)} %fusion.3, bf16[1024,2048]{1,0:T(8,128)(2,1)S(1)} %copy-done.4, bf16[704,2048]{1,0:T(8,128)(2,1)S(1)} %copy-done.7), kind=kOutput, calls=%fused_computation.5 | convolution fusion | flops 2962161664 | bytes 15728640 | tf_op jit(solution)/shard_map/dot_general | solution.py:21
  98.9 0.0 copy-start.9
  98.9 0.0 copy-start.8
  98.9 4.7 %convolution_convert_fusion.2.refs_3_ = bf16[704,2048]{1,0:T(8,128)(2,1)} fusion(bf16[1024,2048]{1,0:T(8,128)(2,1)S(1)} %copy-done.4, f32[1024,704]{0,1:T(8,128)S(1)} %fusion.3, f32[1024,704]{0,1:T(8,128)S(1)} %fusion.4), kind=kOutput, calls=%fused_computation.3 | convolution fusion | flops 2958557184 | bytes 12845056 | tf_op jit(solution)/shard_map/dot_general | solution.py:15
  103.6 0.0 copy-done.9
  103.6 3.4 %convolution_convert_fusion = bf16[2048,704]{0,1:T(8,128)(2,1)S(1)} fusion(bf16[1024,704]{0,1:T(8,128)(2,1)S(1)} %get-tuple-element.22, bf16[1024,2048]{1,0:T(8,128)(2,1)S(1)} %copy-done.3), kind=kOutput, calls=%fused_computation.1 | convolution fusion | flops 2954231808 | bytes 8519680 | tf_op jit(solution)/shard_map/dot_general | solution.py:15
  107.0 0.0 copy-done.8
  107.0 4.7 %convolution_convert_fusion.1 = bf16[2048,704]{0,1:T(8,128)(2,1)} fusion(bf16[1024,704]{0,1:T(8,128)(2,1)S(1)} %get-tuple-element.23, bf16[1024,2048]{1,0:T(8,128)(2,1)S(1)} %copy-done.3), kind=kOutput, calls=%fused_computation.2 | convolution fusion | flops 2954231808 | bytes 8519680 | tf_op jit(solution)/shard_map/dot_general | solution.py:15
  111.6 4.6 %copy.17.refs_1_ = bf16[2048,704]{1,0:T(8,128)(2,1)} copy(bf16[2048,704]{0,1:T(8,128)(2,1)} %convolution_convert_fusion.1) | data formatting | bytes 5767168 | tf_op jit(solution)/shard_map/convert_element_type | solution.py:17
  116.3 2.8 %copy.18.refs_2_ = bf16[2048,704]{1,0:T(8,128)(2,1)} copy(bf16[2048,704]{0,1:T(8,128)(2,1)S(1)} %convolution_convert_fusion) | data formatting | bytes 5767168 | tf_op jit(solution)/shard_map/convert_element_type | solution.py:17
  119.1 6.0 %fusion.5 = f32[1024,2048]{1,0:T(8,128)S(1)} fusion(bf16[1024,704]{0,1:T(8,128)(2,1)} %copy-done.8, bf16[2048,704]{1,0:T(8,128)(2,1)} %get-tuple-element.13), kind=kOutput, calls=%fused_computation.12 | convolution fusion | flops 2952790016 | bytes 12713984 | tf_op jit(solution)/shard_map/dot_general | solution.py:21
  125.1 0.0 copy-done.5
  125.1 0.0 copy-done.10
  125.1 5.2 %add_convert_fusion.refs_0_ = bf16[1024,2048]{1,0:T(8,128)(2,1)} fusion(f32[1024,2048]{1,0:T(8,128)S(1)} %fusion.5, bf16[1024,704]{0,1:T(8,128)(2,1)S(1)} %copy-done.10, bf16[2048,704]{1,0:T(8,128)(2,1)S(1)} %copy-done.5), kind=kOutput, calls=%fused_computation | convolution fusion | flops 2956984320 | bytes 16908288 | tf_op jit(solution)/shard_map/dot_general | solution.py:21
  130.3 130.3 %scatter.1 = (bf16[128,2048]{1,0:T(8,128)(2,1)}, f32[512,704]{1,0:T(8,128)}, f32[512,704]{1,0:T(8,128)}, f32[704,512]{1,0:T(8,128)}) custom-call(bf16[1024,2048]{1,0:T(8,128)(2,1)} %add_convert_fusion.refs_0_, bf16[2048,704]{1,0:T(8,128)(2,1)} %copy.17.refs_1_, bf16[2048,704]{1,0:T(8,128)(2,1)} %copy.18.refs_2_, ...), custom_call_target="tpu_custom_call" | custom-call | tf_op jit(solution)/shard_map/scatter/pallas_call | solution.py:452
  260.6 3.1 %copy.19 = f32[512,704]{0,1:T(8,128)} copy(f32[512,704]{1,0:T(8,128)} %get-tuple-element.19) | data formatting | bytes 2883584 | tf_op jit(solution)/shard_map/scatter/pallas_call | solution.py:452
  263.7 1.6 copy.20
  265.3 0.8 copy.23
  266.1 1.1 copy.24
  (8 shorter events, 0.0 us)
Async XLA Ops:
  85.4 6.1 %copy-start.3 = (bf16[1024,2048]{1,0:T(8,128)(2,1)S(1)}, bf16[1024,2048]{1,0:T(8,128)(2,1)}, u32[]{:S(2)}) copy-start(bf16[1024,2048]{1,0:T(8,128)(2,1)} %get-tuple-element.11) | copy-start | bytes 12582916
  85.4 6.1 %copy-start.6 = (bf16[2048,704]{1,0:T(8,128)(2,1)S(1)}, bf16[2048,704]{1,0:T(8,128)(2,1)}, u32[]{:S(2)}) copy-start(bf16[2048,704]{1,0:T(8,128)(2,1)} %get-tuple-element.13) | copy-start | bytes 8650756
  91.5 3.3 %copy-start.4 = (bf16[1024,2048]{1,0:T(8,128)(2,1)S(1)}, bf16[1024,2048]{1,0:T(8,128)(2,1)}, u32[]{:S(2)}) copy-start(bf16[1024,2048]{1,0:T(8,128)(2,1)} %get-tuple-element.9) | copy-start | bytes 12582916
  91.5 3.3 %copy-start.7 = (bf16[704,2048]{1,0:T(8,128)(2,1)S(1)}, bf16[704,2048]{1,0:T(8,128)(2,1)}, u32[]{:S(2)}) copy-start(bf16[704,2048]{1,0:T(8,128)(2,1)} %get-tuple-element.10) | copy-start | bytes 8650756
  98.9 4.7 %copy-start.9 = (bf16[1024,704]{0,1:T(8,128)(2,1)}, bf16[1024,704]{0,1:T(8,128)(2,1)S(1)}, u32[]{:S(2)}) copy-start(bf16[1024,704]{0,1:T(8,128)(2,1)S(1)} %get-tuple-element.22) | copy-start | bytes 4325380
  98.9 8.0 %copy-start.8 = (bf16[1024,704]{0,1:T(8,128)(2,1)}, bf16[1024,704]{0,1:T(8,128)(2,1)S(1)}, u32[]{:S(2)}) copy-start(bf16[1024,704]{0,1:T(8,128)(2,1)S(1)} %get-tuple-element.23) | copy-start | bytes 4325380
  119.1 6.0 %copy-start.5 = (bf16[2048,704]{1,0:T(8,128)(2,1)S(1)}, bf16[2048,704]{1,0:T(8,128)(2,1)}, u32[]{:S(2)}) copy-start(bf16[2048,704]{1,0:T(8,128)(2,1)} %get-tuple-element.12) | copy-start | bytes 8650756
  119.1 6.0 %copy-start.10 = (bf16[1024,704]{0,1:T(8,128)(2,1)S(1)}, bf16[1024,704]{0,1:T(8,128)(2,1)}, u32[]{:S(2)}) copy-start(bf16[1024,704]{0,1:T(8,128)(2,1)} %copy-done.9) | copy-start | bytes 4325380
  260.6 3.1 %copy-start = (f32[512,704]{1,0:T(8,128)S(1)}, f32[512,704]{1,0:T(8,128)}, u32[]{:S(2)}) copy-start(f32[512,704]{1,0:T(8,128)} %get-tuple-element.20) | copy-start | bytes 4325380
  260.6 4.7 %copy-start.2 = (bf16[128,2048]{1,0:T(8,128)(2,1)S(1)}, bf16[128,2048]{1,0:T(8,128)(2,1)}, u32[]{:S(2)}) copy-start(bf16[128,2048]{1,0:T(8,128)(2,1)} %get-tuple-element.28) | copy-start | bytes 1572868
  260.6 5.5 %copy-start.1 = (f32[704,512]{1,0:T(8,128)S(1)}, f32[704,512]{1,0:T(8,128)}, u32[]{:S(2)}) copy-start(f32[704,512]{1,0:T(8,128)} %get-tuple-element.31) | copy-start | bytes 4325380

commit v2 on v1

--- a/solution.py
+++ b/solution.py
@@ -63,20 +63,15 @@
     z = tp // CORES
     orders = orders_of(n_fs)
     phases = len(orders[0])
-    weights = ((ins[1], outs[1], 0), (ins[2], outs[2], 0), (ins[3], outs[3], 1))
+    weights = tuple((ins[i], outs[i]) for i in (1, 2, 3))
     rows = ((ins[0], outs[0]), (ins[4], outs[4]))
     greet(n_fs, depth, fs, tp, z)
 
     def w_block(array, split, owner):
-        ref, out, axis = weights[array]
-        half = ref.shape[0] // 2
-        if axis == 0:
-            own = ref.at[pl.ds(split * half, half), :]
-            there = out.at[pl.ds(pl.multiple_of(owner * ref.shape[0] + split * half, half), half), :]
-        else:
-            own = ref.at[pl.ds(split * half, half), :]
-            cols = ref.shape[1]
-            there = out.at[pl.ds(split * half, half), pl.ds(pl.multiple_of(owner * cols, cols), cols)]
+        ref, out = weights[array]
+        half, cols = ref.shape[0] // 2, ref.shape[1]
+        own = ref.at[pl.ds(split * half, half), :]
+        there = out.at[pl.ds(split * half, half), pl.ds(pl.multiple_of(owner * cols, cols), cols)]
         return own, there
 
     def w_copy(array, split, phase, mask):
@@ -232,8 +227,8 @@
         functools.partial(gather_kernel, n_fs, n_tp),
         out_shape=(
             full(tokens, 0, n_tp),
-            full(gate, 0, n_fs),
-            full(up, 0, n_fs),
+            full(gate, 1, n_fs),
+            full(up, 1, n_fs),
             full(down, 1, n_fs),
             full(cot, 0, n_tp),
         ),
@@ -264,18 +259,13 @@
     z, core = tp // CORES, tp % CORES
     orders = orders_of(n_fs)
     phases = len(orders[0])
-    axes = (0, 0, 1)
     f32 = jnp.float32
     greet(n_fs, depth, fs, tp, z)
 
     def w_own(array, split, mask):
-        out, axis = w_outs[array], axes[array]
-        half = out.shape[0] // 2
+        out = w_outs[array]
+        half, cols = out.shape[0] // 2, out.shape[1]
         owner = fs ^ mask
-        if axis == 0:
-            start = pl.multiple_of(owner * out.shape[0] + split * half, half)
-            return w_refs[array].at[pl.ds(start, half), :]
-        cols = out.shape[1]
         return w_refs[array].at[
             pl.ds(split * half, half), pl.ds(pl.multiple_of(owner * cols, cols), cols)
         ]
@@ -404,12 +394,8 @@
     z_events = [
         functools.partial(z_event, way, step) for step in range(depth - 1) for way in range(2)
     ]
-    per = -(-len(z_events) // max(len(w_events), 1))
-    for i in range(max(len(w_events), -(-len(z_events) // per))):
-        for event in z_events[i * per : (i + 1) * per]:
-            event()
-        if i < len(w_events):
-            w_events[i]()
+    for event in z_events + w_events:
+        event()
 
     total = both[z].astype(f32)
     zero = jnp.zeros_like(total)
@@ -442,11 +428,7 @@
     f32 = jnp.float32
     vmem = pl.BlockSpec(memory_space=pltpu.VMEM)
     dma = pltpu.SemaphoreType.DMA
-    shapes = (
-        (gg.shape[0] // n_fs, gg.shape[1]),
-        (gu.shape[0] // n_fs, gu.shape[1]),
-        (gd.shape[0], gd.shape[1] // n_fs),
-    )
+    shapes = tuple((g.shape[0], g.shape[1] // n_fs) for g in (gg, gu, gd))
     n, width = gi.shape[0] // n_tp, gi.shape[1]
     slots = [pltpu.VMEM((2, n_fs - 1, s[0] // 2, s[1]), gi.dtype) for s in shapes]
     return pl.pallas_call(
@@ -478,25 +460,27 @@
 def body(n_fs, n_tp, tokens, gate_weight, up_weight, down_weight, grad_out):
     bf16 = tokens.dtype
     tok_all, gate_full, up_full, down_full, cot_all = gather_all(
-        n_fs, n_tp, tokens, gate_weight, up_weight, down_weight, grad_out
+        n_fs, n_tp, tokens, gate_weight.T, up_weight.T, down_weight, grad_out
     )
-    gate_pre = jnp.dot(tok_all, gate_full, preferred_element_type=jnp.float32)
-    up_pre = jnp.dot(tok_all, up_full, preferred_element_type=jnp.float32)
+    gate_pre = over_cols(tok_all, gate_full)
+    up_pre = over_cols(tok_all, up_full)
     sig_gate = jax.nn.sigmoid(gate_pre)
     active = gate_pre * sig_gate
     hidden = (active * up_pre).astype(bf16)
     d_hidden = over_cols(cot_all, down_full)
     d_gate = (d_hidden * up_pre * sig_gate * (1.0 + gate_pre * (1.0 - sig_gate))).astype(bf16)
     d_up = (d_hidden * active).astype(bf16)
-    grad_input = (over_cols(d_gate, gate_full) + over_cols(d_up, up_full)).astype(bf16)
-    return scatter_all(
+    dot = functools.partial(jnp.dot, preferred_element_type=jnp.float32)
+    grad_input = (dot(d_gate, gate_full) + dot(d_up, up_full)).astype(bf16)
+    grad_input, grad_gate, grad_up, grad_down = scatter_all(
         n_fs,
         n_tp,
         grad_input,
-        over_rows(tok_all, d_gate, bf16),
-        over_rows(tok_all, d_up, bf16),
+        over_rows(d_gate, tok_all, bf16),
+        over_rows(d_up, tok_all, bf16),
         over_rows(hidden, cot_all, bf16),
     )
+    return grad_input, grad_gate.T, grad_up.T, grad_down
 
 
 def solution(mesh):

time: 267 us -> 250 us (0.936)
  local copies, waits for them, and re-layouts: 18.6 us -> 6.9 us
  Pallas kernels: 210 us -> 206 us
    convert_element_type x2 -> x0, local copies, waits for them, and re-layouts: 7.46 us -> none  [over_rows(): return lax.dot_general(left, right, (((0,), (0,)), ((), ())), preferred_e...]
    pallas_call x2 -> x0, local copies, waits for them, and re-layouts: 4.66 us -> none  [scatter_all(): pl.pallas_call(functools.partial(scatter_kernel, n_fs, n_tp), out_shape=(...]
    pallas_call x1, Pallas kernels: 80.2 us -> 76 us  [gather_all(): pl.pallas_call(functools.partial(gather_kernel, n_fs, n_tp), out_shape=(f...]
    unnamed x26 -> x18, local copies, waits for them, and re-layouts: 6.47 us -> 6.9 us
where the time goes in v2:
time: 250 us
  Pallas kernels  206 us (82%)
  matrix products  35.8 us (14%)
  local copies, waits for them, and re-layouts  6.9 us (3%)
    pallas_call x1, Pallas kernels, scatter_all(): pl.pallas_call(functools.partial(scatter_kernel, n_fs, n_tp), out_shape=(...  130 us
    pallas_call x1, Pallas kernels, gather_all(): pl.pallas_call(functools.partial(gather_kernel, n_fs, n_tp), out_shape=(f...  76 us
    dot_general x3, matrix products, over_rows(): lax.dot_general(left, right, (((0,), (0,)), ((), ())), preferred_element_...  13.7 us
    dot_general x3, matrix products, over_cols(): lax.dot_general(left, right, (((1,), (1,)), ((), ())), preferred_element_...  13.2 us
    dot_general x2, matrix products, body(): grad_input = (dot(d_gate, gate_full) + dot(d_up, up_full)).astype(bf16)  8.88 us
    unnamed x18, local copies, waits for them, and re-layouts  6.9 us

profile of v2, /device:TPU:8, one launch (start us, length us, event | category | flops | bytes accessed | tf_op | source)
XLA Modules:
  0.0 249.8 jit_solution(8169199555894832147)
XLA Ops:
  0.6 76.0 %gather.1 = (bf16[1024,2048]{1,0:T(8,128)(2,1)}, bf16[704,2048]{1,0:T(8,128)(2,1)}, bf16[704,2048]{1,0:T(8,128)(2,1)}, bf16[704,2048]{1,0:T(8,128)(2,1)}, bf16[1024,2048]{1,0:T(8,128)(2,1)}) custom-call(bf16[128,2048]{1,0:T(8,128)(2,1)} %refs_0_.1, bf16[704,512]{1,0:T(8,128)(2,1)} %bitcast.21, bf16[704,512]{1,0:T(8,128)(2,1)} %bitcast.22, ...), custom_call_target="tpu_custom_call" | custom-call | tf_op jit(solution)/shard_map/gather/pallas_call | solution.py:226
  76.6 0.0 copy-start.2
  76.6 0.0 copy-start.5
  76.6 6.0 %fusion.3 = f32[1024,704]{0,1:T(8,128)S(1)} fusion(bf16[1024,2048]{1,0:T(8,128)(2,1)} %get-tuple-element.15, bf16[704,2048]{1,0:T(8,128)(2,1)} %get-tuple-element.16), kind=kOutput, calls=%fused_computation.10 | convolution fusion | flops 2952790016 | bytes 9961472 | tf_op jit(solution)/shard_map/dot_general | solution.py:21
  82.7 0.0 copy-done.2
  82.7 0.0 copy-done.5
  82.7 0.0 copy-start.3
  82.7 0.0 copy-start.6
  82.7 3.2 %fusion.4 = f32[1024,704]{0,1:T(8,128)S(1)} fusion(bf16[1024,2048]{1,0:T(8,128)(2,1)S(1)} %copy-done.2, bf16[704,2048]{1,0:T(8,128)(2,1)S(1)} %copy-done.5), kind=kOutput, calls=%fused_computation.11 | convolution fusion | flops 2952790016 | bytes 9961472 | tf_op jit(solution)/shard_map/dot_general | solution.py:21
  85.9 0.0 copy-done.3
  85.9 0.0 copy-done.6
  85.9 4.0 %multiply_convert_fusion.1 = (bf16[1024,704]{0,1:T(8,128)(2,1)S(1)}, bf16[1024,704]{0,1:T(8,128)(2,1)S(1)}) fusion(f32[1024,704]{0,1:T(8,128)S(1)} %fusion.4, f32[1024,704]{0,1:T(8,128)S(1)} %fusion.3, bf16[1024,2048]{1,0:T(8,128)(2,1)S(1)} %copy-done.3, bf16[704,2048]{1,0:T(8,128)(2,1)S(1)} %copy-done.6), kind=kOutput, calls=%fused_computation.5 | convolution fusion | flops 2962161664 | bytes 15728640 | tf_op jit(solution)/shard_map/dot_general | solution.py:21
  89.9 4.7 %convolution_convert_fusion.refs_3_ = bf16[704,2048]{1,0:T(8,128)(2,1)} fusion(bf16[1024,2048]{1,0:T(8,128)(2,1)S(1)} %copy-done.3, f32[1024,704]{0,1:T(8,128)S(1)} %fusion.3, f32[1024,704]{0,1:T(8,128)S(1)} %fusion.4), kind=kOutput, calls=%fused_computation.1 | convolution fusion | flops 2958557184 | bytes 12845056 | tf_op jit(solution)/shard_map/dot_general | solution.py:15
  94.6 4.5 %convolution_convert_fusion.1.refs_2_ = bf16[704,2048]{1,0:T(8,128)(2,1)} fusion(bf16[1024,704]{0,1:T(8,128)(2,1)S(1)} %get-tuple-element.22, bf16[1024,2048]{1,0:T(8,128)(2,1)S(1)} %copy-done.2), kind=kOutput, calls=%fused_computation.2 | convolution fusion | flops 2954231808 | bytes 8519680 | tf_op jit(solution)/shard_map/dot_general | solution.py:15
  99.2 4.5 %convolution_convert_fusion.2.refs_1_ = bf16[704,2048]{1,0:T(8,128)(2,1)} fusion(bf16[1024,704]{0,1:T(8,128)(2,1)S(1)} %get-tuple-element.23, bf16[1024,2048]{1,0:T(8,128)(2,1)S(1)} %copy-done.2), kind=kOutput, calls=%fused_computation.3 | convolution fusion | flops 2954231808 | bytes 8519680 | tf_op jit(solution)/shard_map/dot_general | solution.py:15
  103.7 0.0 copy-start.4
  103.7 3.5 %fusion.5 = f32[1024,2048]{1,0:T(8,128)S(1)} fusion(bf16[1024,704]{0,1:T(8,128)(2,1)S(1)} %get-tuple-element.23, bf16[704,2048]{1,0:T(8,128)(2,1)S(1)} %copy-done.5), kind=kOutput, calls=%fused_computation.12 | convolution fusion | flops 2952790016 | bytes 12713984 | tf_op jit(solution)/shard_map/dot_general | solution.py:474
  107.2 0.0 copy-done.4
  107.2 5.4 %add_convert_fusion.refs_0_ = bf16[1024,2048]{1,0:T(8,128)(2,1)} fusion(f32[1024,2048]{1,0:T(8,128)S(1)} %fusion.5, bf16[1024,704]{0,1:T(8,128)(2,1)S(1)} %get-tuple-element.22, bf16[704,2048]{1,0:T(8,128)(2,1)S(1)} %copy-done.4), kind=kOutput, calls=%fused_computation | convolution fusion | flops 2956984320 | bytes 16908288 | tf_op jit(solution)/shard_map/dot_general | solution.py:474
  112.6 130.4 %scatter.1 = (bf16[128,2048]{1,0:T(8,128)(2,1)}, f32[704,512]{1,0:T(8,128)}, f32[704,512]{1,0:T(8,128)}, f32[704,512]{1,0:T(8,128)}) custom-call(bf16[1024,2048]{1,0:T(8,128)(2,1)} %add_convert_fusion.refs_0_, bf16[704,2048]{1,0:T(8,128)(2,1)} %convolution_convert_fusion.2.refs_1_, bf16[704,2048]{1,0:T(8,128)(2,1)} %convolution_convert_fusion.1.refs_2_, ...), custom_call_target="tpu_custom_call" | custom-call | tf_op jit(solution)/shard_map/scatter/pallas_call | solution.py:434
  243.0 0.0 copy-start.1
  243.0 2.0 copy.13
  245.0 0.0 copy-start
  245.0 2.7 %copy.14 = f32[512,704]{0,1:T(8,128)} copy(f32[512,704]{0,1:T(8,128)} %bitcast.20) | data formatting | bytes 2883584
  247.6 0.0 copy-done.1
  247.6 1.1 copy.15
  248.7 0.0 copy-done
  248.7 1.1 copy.16
Async XLA Ops:
  76.6 6.0 %copy-start.2 = (bf16[1024,2048]{1,0:T(8,128)(2,1)S(1)}, bf16[1024,2048]{1,0:T(8,128)(2,1)}, u32[]{:S(2)}) copy-start(bf16[1024,2048]{1,0:T(8,128)(2,1)} %get-tuple-element.15) | copy-start | bytes 12582916
  76.6 6.0 %copy-start.5 = (bf16[704,2048]{1,0:T(8,128)(2,1)S(1)}, bf16[704,2048]{1,0:T(8,128)(2,1)}, u32[]{:S(2)}) copy-start(bf16[704,2048]{1,0:T(8,128)(2,1)} %get-tuple-element.17) | copy-start | bytes 8650756
  82.7 3.2 %copy-start.3 = (bf16[1024,2048]{1,0:T(8,128)(2,1)S(1)}, bf16[1024,2048]{1,0:T(8,128)(2,1)}, u32[]{:S(2)}) copy-start(bf16[1024,2048]{1,0:T(8,128)(2,1)} %get-tuple-element.13) | copy-start | bytes 12582916
  82.7 3.2 %copy-start.6 = (bf16[704,2048]{1,0:T(8,128)(2,1)S(1)}, bf16[704,2048]{1,0:T(8,128)(2,1)}, u32[]{:S(2)}) copy-start(bf16[704,2048]{1,0:T(8,128)(2,1)} %get-tuple-element.14) | copy-start | bytes 8650756
  103.7 3.5 %copy-start.4 = (bf16[704,2048]{1,0:T(8,128)(2,1)S(1)}, bf16[704,2048]{1,0:T(8,128)(2,1)}, u32[]{:S(2)}) copy-start(bf16[704,2048]{1,0:T(8,128)(2,1)} %get-tuple-element.16) | copy-start | bytes 8650756
  243.0 4.7 %copy-start.1 = (f32[704,512]{1,0:T(8,128)S(1)}, f32[704,512]{1,0:T(8,128)}, u32[]{:S(2)}) copy-start(f32[704,512]{1,0:T(8,128)} %get-tuple-element.20) | copy-start | bytes 4325380
  245.0 3.8 %copy-start = (f32[704,512]{1,0:T(8,128)S(1)}, f32[704,512]{1,0:T(8,128)}, u32[]{:S(2)}) copy-start(f32[704,512]{1,0:T(8,128)} %get-tuple-element.31) | copy-start | bytes 4325380
